TPU v7x, 32 devices: a whole 2x2x4 slice. The times are simulated.
32 devices in a mesh: kv: 16 (over z, y, x), tp: 2 (over core).
Axes of the slice: x: 2, y: 2, z: 4, core: 2. Of those that a mesh axis runs over, the one named last changes fastest.
Arguments:
- tokens: bfloat16 [16, 4096], P(None, ('kv', 'tp')), may hold values from -12 to 12
- lengths: int32 [16], replicated, may hold values from 1 to 2048, 10922 in all
- attn_gain: bfloat16 [4096], P('kv'), may hold values from 0.099609375 to 1.8984375
- w_query: bfloat16 [4096, 2048], P('kv', 'tp'), may hold values from -0.09375 to 0.09375
- w_key: bfloat16 [4096, 2048], P('kv', 'tp'), may hold values from -0.09375 to 0.09375
- w_value: bfloat16 [4096, 4096], P('kv', 'tp'), may hold values from -0.09375 to 0.09375
- w_gate: bfloat16 [4096, 4096], P('kv', 'tp'), may hold values from -0.09375 to 0.09375
- decay_rate: float32 [32], P('tp'), may hold values from 4.8828125e-05 to 0.05
- key_cache: bfloat16 [16, 2048, 2048], P(None, 'kv', 'tp'), may hold values from -6 to 6
- value_cache: bfloat16 [16, 2048, 4096], P(None, 'kv', 'tp'), may hold values from -6 to 6
- head_gain: bfloat16 [4096], P('tp'), may hold values from 0.099609375 to 1.8984375
- w_output: bfloat16 [4096, 4096], P('tp', 'kv'), may hold values from -0.09375 to 0.09375
- mlp_gain: bfloat16 [4096], replicated, may hold values from 0.099609375 to 1.8984375
- w_up: bfloat16 [4096, 16384], P(None, ('kv', 'tp')), may hold values from -0.09375 to 0.09375
- w_down: bfloat16 [16384, 4096], P(('kv', 'tp')), may hold values from -0.09375 to 0.09375
Outputs:
- layer_out: bfloat16 [16, 4096], P(None, ('kv', 'tp'))
Inputs may be any that keep to these rules, and one draw needn't show every extreme that they name: Sequence s has lengths[s] live cache positions, 0 to lengths[s] - 1, and its new token stands at position lengths[s]; the longest fills all 2048 positions.
All inputs are finite; a program needn't handle non-finite values.
Results may differ from a plain program's by a relative error of at most 0.012.
Values may be sent and summed in bfloat16 or wider, within the bound.
A program may use at most 64 MiB of HBM per device.

v0:
```python
import jax
import jax.numpy as jnp
from jax import lax
from jax.sharding import PartitionSpec as P

WIDTH = 4096
HEAD_KEY = 64
HEAD_VALUE = 128
EPS = 1e-05
THETA = 10000.0


def rotate(flattened, position):
    row_count = flattened.shape[0]
    grouped = flattened.reshape(row_count, -1, HEAD_KEY)
    halfway = HEAD_KEY // 2
    inverse = jnp.power(THETA, -jnp.arange(halfway, dtype=jnp.float32) / halfway)
    angles = position.astype(jnp.float32)[:, None] * inverse[None, :]
    cosine = jnp.cos(angles)[:, None, :]
    sine_part = jnp.sin(angles)[:, None, :]
    first_half = grouped[..., :halfway]
    second_half = grouped[..., halfway:]
    turned = jnp.concatenate(
        [
            first_half * cosine - second_half * sine_part,
            second_half * cosine + first_half * sine_part,
        ],
        -1,
    )
    return turned.reshape(row_count, -1)


def affine(product_sum, column, average, inverse_std):
    return inverse_std[:, None] * (product_sum - average[:, None] * column[None, :])


def on_device(
    tokens,
    lengths,
    attn_gain,
    w_query,
    w_key,
    w_value,
    w_gate,
    decay_rate,
    key_cache,
    value_cache,
    head_gain,
    w_output,
    mlp_gain,
    w_up,
    w_down,
):
    seq_count = tokens.shape[0]
    head_count = decay_rate.shape[0]
    span_rows = key_cache.shape[1]
    block_cols = lax.all_gather(tokens, "tp", axis=1, tiled=True)
    widened = block_cols.astype(jnp.float32)
    scaled = (widened * attn_gain.astype(jnp.float32)).astype(jnp.bfloat16)
    gain_row = attn_gain[None, :]
    part_query = jnp.dot(scaled, w_query, preferred_element_type=jnp.float32)
    part_key = jnp.dot(scaled, w_key, preferred_element_type=jnp.float32)
    part_value = jnp.dot(scaled, w_value, preferred_element_type=jnp.float32)
    part_gate = jnp.dot(scaled, w_gate, preferred_element_type=jnp.float32)
    col_query = jnp.dot(gain_row, w_query, preferred_element_type=jnp.float32)[0]
    col_key = jnp.dot(gain_row, w_key, preferred_element_type=jnp.float32)[0]
    col_value = jnp.dot(gain_row, w_value, preferred_element_type=jnp.float32)[0]
    col_gate = jnp.dot(gain_row, w_gate, preferred_element_type=jnp.float32)[0]
    (
        sum_query,
        sum_key,
        sum_value,
        sum_gate,
        csum_query,
        csum_key,
        csum_value,
        csum_gate,
        first_moment,
        second_moment,
    ) = lax.psum(
        (
            part_query,
            part_key,
            part_value,
            part_gate,
            col_query,
            col_key,
            col_value,
            col_gate,
            jnp.sum(widened, -1),
            jnp.sum(widened * widened, -1),
        ),
        "kv",
    )
    average = first_moment / WIDTH
    inverse_std = lax.rsqrt(second_moment / WIDTH - average * average + EPS)
    query_rows = rotate(affine(sum_query, csum_query, average, inverse_std), lengths).astype(
        jnp.bfloat16
    )
    new_key = rotate(affine(sum_key, csum_key, average, inverse_std), lengths).astype(jnp.bfloat16)
    new_value = affine(sum_value, csum_value, average, inverse_std).astype(jnp.bfloat16)
    gate_value = affine(sum_gate, csum_gate, average, inverse_std)
    queries = query_rows.reshape(seq_count, head_count, HEAD_KEY)
    keys_local = key_cache.reshape(seq_count, span_rows, head_count, HEAD_KEY)
    values_local = value_cache.reshape(seq_count, span_rows, head_count, HEAD_VALUE)
    scores = jnp.einsum(
        "bhd,bjhd->bhj", queries, keys_local, preferred_element_type=jnp.float32
    ) * HEAD_KEY ** (-0.5)
    places = lax.axis_index("kv") * span_rows + jnp.arange(span_rows, dtype=jnp.int32)
    distance = jnp.maximum(lengths[:, None] - places[None, :], 0).astype(jnp.float32)
    live_mask = (places[None, :] < lengths[:, None])[:, None, :]
    weights = jnp.where(live_mask, jnp.exp(-decay_rate[None, :, None] * distance[:, None, :]), 0.0)
    coefficients = (scores * weights).astype(jnp.bfloat16)
    partial_out = jnp.einsum(
        "bhj,bjhe->bhe", coefficients, values_local, preferred_element_type=jnp.float32
    )
    cached = lax.psum(partial_out, "kv")
    own_score = jnp.sum(
        queries.astype(jnp.float32)
        * new_key.reshape(seq_count, head_count, HEAD_KEY).astype(jnp.float32),
        -1,
    ) * HEAD_KEY ** (-0.5)
    retained = cached + own_score[:, :, None] * new_value.reshape(
        seq_count, head_count, HEAD_VALUE
    ).astype(jnp.float32)
    centered = retained - jnp.mean(retained, -1, keepdims=True)
    normed = (
        centered
        * lax.rsqrt(jnp.mean(centered * centered, -1, keepdims=True) + EPS)
        * head_gain.reshape(head_count, HEAD_VALUE).astype(jnp.float32)
    )
    gated_out = (jax.nn.silu(gate_value) * normed.reshape(seq_count, -1)).astype(jnp.bfloat16)
    partial_branch = jnp.dot(gated_out, w_output, preferred_element_type=jnp.float32)
    branch = lax.psum_scatter(
        partial_branch.astype(jnp.bfloat16), "tp", scatter_dimension=1, tiled=True
    ).astype(jnp.float32)
    own_residual = (tokens.astype(jnp.float32) + branch).astype(jnp.bfloat16)
    piece_wide = lax.all_gather(own_residual, ("kv", "tp"), axis=1, tiled=True).astype(jnp.float32)
    scaled_piece = (piece_wide * mlp_gain.astype(jnp.float32)).astype(jnp.bfloat16)
    totals = (
        jnp.dot(scaled_piece, w_up, preferred_element_type=jnp.float32),
        jnp.sum(piece_wide, -1),
        jnp.sum(piece_wide * piece_wide, -1),
    )
    accumulated, first_sum, second_sum = totals
    mid_average = first_sum / WIDTH
    mid_inverse = lax.rsqrt(second_sum / WIDTH - mid_average * mid_average + EPS)
    column_up = jnp.dot(mlp_gain[None, :], w_up, preferred_element_type=jnp.float32)[0]
    hidden = jnp.square(
        jax.nn.relu(affine(accumulated, column_up, mid_average, mid_inverse))
    ).astype(jnp.bfloat16)
    down_terms = jnp.dot(hidden, w_down, preferred_element_type=jnp.float32)
    kv_block = lax.psum_scatter(down_terms, "kv", scatter_dimension=1, tiled=True)
    mixer_sum = lax.psum_scatter(kv_block, "tp", scatter_dimension=1, tiled=True)
    return (own_residual.astype(jnp.float32) + mixer_sum).astype(jnp.bfloat16)


def solution(mesh):
    in_specs = (
        P(None, ("kv", "tp")),
        P(),
        P("kv"),
        P("kv", "tp"),
        P("kv", "tp"),
        P("kv", "tp"),
        P("kv", "tp"),
        P("tp"),
        P(None, "kv", "tp"),
        P(None, "kv", "tp"),
        P("tp"),
        P("tp", "kv"),
        P(),
        P(None, ("kv", "tp")),
        P(("kv", "tp"), None),
    )
    out_specs = P(None, ("kv", "tp"))
    return jax.shard_map(
        on_device, mesh=mesh, in_specs=in_specs, out_specs=out_specs, check_vma=False
    )
```

profile of v0, /device:TPU:0, one launch (start us, length us, event | category | flops | bytes accessed | tf_op | source)
XLA Modules:
  0.0 387.7 jit_solution(13604022745507007239)
XLA Ops:
  6.5 2.3 all_gather.6
  8.9 0.7 convert_element_type.87
  9.5 1.8 fusion.36
  11.5 0.1 fusion.25
  11.6 0.7 reshape.195
  12.2 0.7 convert_element_type.89
  12.9 0.7 maximum_convert_fusion
  13.6 0.7 broadcast_compare_fusion
  14.4 1.2 fusion.44
  15.6 0.2 fusion.46
  15.8 0.9 fusion.32
  16.7 1.5 fusion.43
  18.2 0.9 fusion.38
  19.1 0.2 fusion.45
  19.3 0.8 fusion.34
  20.1 0.1 multiply_cosine_fusion
  20.2 78.5 %all-reduce = (f32[1024]{0:T(1024)S(1)}, f32[16]{0:T(128)S(1)}, f32[16]{0:T(128)S(1)}, f32[2048]{0:T(1024)S(1)}, f32[1024]{0:T(1024)S(1)}, /*index=5*/f32[2048]{0:T(1024)S(1)}) all-reduce(f32[1024]{0:T(1024)S(1)} %bitcast.62, f32[16]{0:T(128)S(1)} %get-tuple-element.8, ...), channel_id=1, replica_groups=mesh['kv'=16,'tp'=2] {'kv'}, use_global_device_ids=true, to_apply=%region_7.0 | all-reduce | flops 6176 | bytes 49408 | tf_op jit(solution)/shard_map/psum | solution.py:80
  98.7 6.4 %copy.17 = bf16[16,128,1024]{1,2,0:T(8,128)(2,1)} copy(bf16[16,128,1024]{2,1,0:T(8,128)(2,1)} %param.23) | data formatting | bytes 8388608 | tf_op args[8]
  105.1 13.9 %all-reduce.5.cloned.1.call-done = f32[16,1024]{1,0:T(8,128)} async-done(((f32[16,1024]{1,0:T(8,128)}), f32[16,1024]{1,0:T(8,128)}) %all-reduce.5.cloned.1.call-update) | async-done | bytes 65552 | tf_op jit(solution)/shard_map/psum | solution.py:80
  119.1 0.9 subtract_multiply_fusion.1
  120.0 0.1 reshape.188
  120.1 0.1 subtract_convert_fusion.1
  120.2 0.1 fusion.31
  120.3 3.4 fusion.14
  123.6 0.1 fusion.18
  123.8 6.4 %fusion = f32[16,16,1,128]{3,2,1,0:T(1,128)} fusion(bf16[16,16,128,1]{2,1,0,3:T(8,128)(2,1)S(1)} %fusion.18, bf16[16,128,2048]{2,1,0:T(8,128)(2,1)} %param.24), kind=kOutput, calls=%fused_computation | convolution fusion | flops 8388608 | bytes 8585216 | tf_op jit(solution)/shard_map/bhj,bjhe->bhe/dot_general | solution.py:114
  130.3 109.1 %all-reduce.7.cloned.1.call-done = (f32[16,16,128]{2,1,0:T(8,128)}, f32[16,2048]{1,0:T(8,128)}, f32[16,1024]{1,0:T(8,128)}, f32[16,2048]{1,0:T(8,128)}) async-done(((f32[16,16,128]{2,1,0:T(8,128)}, f32[16,2048]{1,0:T(8,128)}, f32[16,1024]{1,0:T(8,128)}, f32[16,2048]{1,0:T(8,128)}), (f32[16,16,128]{2,1,0:T(8,128)}, f32[16,2048]{1,0:T(8,128)}, f32[16,1024]{1,0:T(8,128)}, ...) | async-done | bytes 458768 | tf_op jit(solution)/shard_map/psum | solution.py:117
  239.5 0.9 subtract_multiply_fusion
  240.4 0.1 reshape.191
  240.5 0.1 subtract_convert_fusion
  240.6 0.2 multiply_reduce_fusion.1
  240.8 1.0 convert_bitcast_fusion
  241.8 0.1 bitcast_multiply_fusion.1
  241.9 1.0 fusion.42
  243.0 0.2 multiply_reduce_fusion
  243.2 0.1 multiply_multiply_fusion
  243.3 1.2 convolution_convert_fusion
  244.5 0.7 copy.23
  245.3 0.0 reduce-scatter.6.cloned.1.call-start
  245.4 2.8 fusion.47
  248.2 3.9 %reduce-scatter.10.cloned.1.call-done = bf16[128,16]{1,0:T(8,128)(2,1)} async-done(((bf16[256,16]{1,0:T(8,128)(2,1)}), bf16[128,16]{1,0:T(8,128)(2,1)}) %reduce-scatter.10.cloned.1.call-update) | async-done | bytes 4112
  252.1 0.8 copy.24
  253.0 42.0 %all_gather.7 = bf16[16,4096]{1,0:T(8,128)(2,1)S(1)} all-gather(bf16[16,128]{1,0:T(8,128)(2,1)S(1)} %add_convert_fusion.3), channel_id=1, replica_groups=mesh['kv'=16,'tp'=2] {'kv','tp'}, dimensions={1}, use_global_device_ids=true | all-gather | bytes 135168 | tf_op jit(solution)/shard_map/all_gather | solution.py:138
  295.0 0.2 fusion.8
  295.1 5.5 %fusion.7 = f32[16,4096]{1,0:T(8,128)} fusion(bf16[512,4096]{1,0:T(8,128)(2,1)} %param.29, bf16[4096,512]{1,0:T(8,128)(2,1)} %param.28, bf16[16,4096]{1,0:T(8,128)(2,1)S(1)} %all_gather.7, f32[4096]{0:T(1024)S(1)} %convert_element_type.105, f32[512]{0:T(512)S(1)} %bitcast.64, f32[16]{0:T(128)S(1)} %get-tuple-element.28, f32[16]{0:T(128)S(1)} %get-tuple-element.27), kind=kOutput, calls=%fused_computation.8 | convolution fusion | flops 134463488 | bytes 8800384 | tf_op jit(solution)/shard_map/dot_general | solution.py:152
  300.7 73.3 %reduce-scatter.6.cloned.1.call-done = f32[16,256]{1,0:T(8,128)} async-done(((f32[16,4096]{1,0:T(8,128)}), f32[16,256]{1,0:T(8,128)}) %reduce-scatter.6.cloned.1.call-update) | async-done | bytes 16400 | tf_op jit(solution)/shard_map/reduce_scatter | solution.py:153
  374.0 5.9 %reduce-scatter.8.cloned.1.call-done = f32[16,128]{1,0:T(8,128)} async-done(((f32[16,256]{1,0:T(8,128)}), f32[16,128]{1,0:T(8,128)}) %reduce-scatter.8.cloned.1.call-update) | async-done | bytes 8208 | tf_op jit(solution)/shard_map/reduce_scatter | solution.py:154
  379.9 1.3 add_convert_fusion.2
  (38 shorter events, 0.4 us)
Async XLA Ops:
  6.5 9.1 %copy-start = (bf16[256,2048]{1,0:T(8,128)(2,1)S(1)}, bf16[256,2048]{1,0:T(8,128)(2,1)}, u32[]{:S(2)}) copy-start(bf16[256,2048]{1,0:T(8,128)(2,1)} %param.20) | copy-start | bytes 3145732
  6.5 11.7 %copy-start.1 = (bf16[256,2048]{1,0:T(8,128)(2,1)S(1)}, bf16[256,2048]{1,0:T(8,128)(2,1)}, u32[]{:S(2)}) copy-start(bf16[256,2048]{1,0:T(8,128)(2,1)} %param.21) | copy-start | bytes 3145732
  6.5 12.6 %copy-start.2 = (bf16[256,1024]{1,0:T(8,128)(2,1)S(1)}, bf16[256,1024]{1,0:T(8,128)(2,1)}, u32[]{:S(2)}) copy-start(bf16[256,1024]{1,0:T(8,128)(2,1)} %param.19) | copy-start | bytes 1572868
  6.5 112.5 %all-reduce.5.cloned.1.call-start = ((), (), s32[]{:S(2)}) async-start(), calls=%async_computation.3 | async-start | bytes 131072 | tf_op jit(solution)/shard_map/psum | solution.py:80
  11.4 228.1 %all-reduce.7.cloned.1.call-start = ((), (), s32[]{:S(2)}) async-start(), calls=%async_computation.7 | async-start | bytes 917504 | tf_op jit(solution)/shard_map/psum | solution.py:117
  98.7 6.4 %copy-start.7 = (f32[16]{0:T(128)S(1)}, f32[16]{0:T(128)}, u32[]{:S(2)}) copy-start(f32[16]{0:T(128)} %param.22) | copy-start | bytes 196
  123.8 6.5 %copy-start.4 = (bf16[4096]{0:T(1024)(128)(2,1)S(1)}, bf16[4096]{0:T(1024)(128)(2,1)}, u32[]{:S(2)}) copy-start(bf16[4096]{0:T(1024)(128)(2,1)} %param.27) | copy-start | bytes 24580
  123.8 6.5 %copy-start.6 = (bf16[2048]{0:T(1024)(128)(2,1)S(1)}, bf16[2048]{0:T(1024)(128)(2,1)}, u32[]{:S(2)}) copy-start(bf16[2048]{0:T(1024)(128)(2,1)} %param.25) | copy-start | bytes 12292
  123.8 119.5 %copy-start.3 = (bf16[2048,256]{1,0:T(8,128)(2,1)S(1)}, bf16[2048,256]{1,0:T(8,128)(2,1)}, u32[]{:S(2)}) copy-start(bf16[2048,256]{1,0:T(8,128)(2,1)} %param.26) | copy-start | bytes 3145732
  130.2 121.9 %reduce-scatter.10.cloned.1.call-start = ((), (), s32[]{:S(2)}) async-start(), calls=%async_computation.6 | async-start | bytes 98304
  240.4 12.6 %copy-start.5 = (bf16[16,128]{1,0:T(8,128)(2,1)S(1)}, bf16[16,128]{1,0:T(8,128)(2,1)}, u32[]{:S(2)}) copy-start(bf16[16,128]{1,0:T(8,128)(2,1)} %param.15) | copy-start | bytes 12292
  245.3 128.7 %reduce-scatter.6.cloned.1.call-start = ((), (), s32[]{:S(2)}) async-start(), calls=%async_computation.4 | async-start | bytes 278528 | tf_op jit(solution)/shard_map/reduce_scatter | solution.py:153
  300.6 79.3 %reduce-scatter.8.cloned.1.call-start = ((), (), s32[]{:S(2)}) async-start(), calls=%async_computation.5 | async-start | bytes 24576 | tf_op jit(solution)/shard_map/reduce_scatter | solution.py:154
Sparse Core Ops, SparseCore 0:
  12.8 106.1 all-reduce.4
  130.4 109.0 all-reduce.6
  245.4 6.6 reduce-scatter.9
  300.7 73.1 reduce-scatter.5
  376.0 3.8 reduce-scatter.7
where the time goes:
time: 388 us
  waiting for transfers between devices  206 us (53%)
  blocking collectives  123 us (32%)
  matrix products  26.8 us (7%)
  between operations  13.3 us (3%)
  other arithmetic  9.4 us (2%)
  local copies, waits for them, and re-layouts  8.86 us (2%)
    psum x1, waiting for transfers between devices, on_device(): cached = lax.psum(partial_out, 'kv')  109 us
    psum x1, blocking collectives, on_device(): lax.psum((part_query, part_key, part_value, part_gate, col_query, col_key...  78.5 us
    reduce_scatter x1, waiting for transfers between devices, on_device(): lax.psum_scatter(down_terms, 'kv', scatter_dimension=1, tiled=True)  73.3 us
    all_gather x1, blocking collectives, on_device(): lax.all_gather(own_residual, ('kv', 'tp'), axis=1, tiled=True)  42 us
    psum x1, waiting for transfers between devices, on_device(): lax.psum((part_query, part_key, part_value, part_gate, col_query, col_key...  13.9 us
    unnamed x22, local copies, waits for them, and re-layouts  8.69 us
  transfers between devices with their start and end apart: 5, of which 5 were waited for; matrix products, arithmetic and copies ran while one was open for 5% of the time, Pallas kernels for 0%

commit v1 on v0

--- a/solution.py
+++ b/solution.py
@@ -114,7 +114,8 @@
     partial_out = jnp.einsum(
         "bhj,bjhe->bhe", coefficients, values_local, preferred_element_type=jnp.float32
     )
-    cached = lax.psum(partial_out, "kv")
+    pieces = lax.all_gather(partial_out, "kv", axis=0, tiled=False)
+    cached = pieces.sum(axis=0)
     own_score = jnp.sum(
         queries.astype(jnp.float32)
         * new_key.reshape(seq_count, head_count, HEAD_KEY).astype(jnp.float32),

time: 388 us -> 346 us (0.89)
  waiting for transfers between devices: 206 us -> 168 us
    psum x1 -> x0, waiting for transfers between devices: 109 us -> none  [on_device(): cached = lax.psum(partial_out, 'kv')]
    all_gather x0 -> x1, waiting for transfers between devices: none -> 59.1 us  [on_device(): pieces = lax.all_gather(partial_out, 'kv', axis=0, tiled=False)]
    psum x1, waiting for transfers between devices: 13.9 us -> 25.6 us  [on_device(): lax.psum((part_query, part_key, part_value, part_gate, col_query, col_key...]
    unnamed x22 -> x30, local copies, waits for them, and re-layouts: 8.69 us -> 8.7 us
  transfers between devices with their start and end apart: 5 -> 5, of which waited for: 5 -> 5; matrix products, arithmetic and copies ran while one was open for 5% -> 3% of each run, Pallas kernels for 0% -> 0%
where the time goes in v1:
time: 346 us; the launch traced here: 345 us
  waiting for transfers between devices  168 us (49%)
  blocking collectives  123 us (36%)
  matrix products  26 us (8%)
  between operations  13.4 us (4%)
  local copies, waits for them, and re-layouts  9.14 us (3%)
  other arithmetic  6.28 us (2%)
    psum x1, blocking collectives, on_device(): lax.psum((part_query, part_key, part_value, part_gate, col_query, col_key...  78.4 us
    reduce_scatter x1, waiting for transfers between devices, on_device(): lax.psum_scatter(down_terms, 'kv', scatter_dimension=1, tiled=True)  73.3 us
    all_gather x1, waiting for transfers between devices, on_device(): pieces = lax.all_gather(partial_out, 'kv', axis=0, tiled=False)  59.1 us
    all_gather x1, blocking collectives, on_device(): lax.all_gather(own_residual, ('kv', 'tp'), axis=1, tiled=True)  42 us
    psum x1, waiting for transfers between devices, on_device(): lax.psum((part_query, part_key, part_value, part_gate, col_query, col_key...  25.6 us
    unnamed x30, local copies, waits for them, and re-layouts  8.7 us
  transfers between devices with their start and end apart: 5, of which 5 were waited for; matrix products, arithmetic and copies ran while one was open for 3% of the time, Pallas kernels for 0%

profile of v1, /device:TPU:0, one launch (start us, length us, event | category | flops | bytes accessed | tf_op | source)
XLA Modules:
  0.0 345.4 jit_solution(12407448499209255228)
XLA Ops:
  6.6 2.3 all_gather.12
  8.9 0.7 convert_element_type.87
  9.6 2.1 fusion.38
  11.7 0.9 fusion.44
  12.6 1.8 fusion.40
  14.5 1.8 fusion.42
  16.3 0.0 all-gather.3.cloned.1.call-start
  16.4 0.1 fusion.31
  16.5 0.7 reshape.195
  17.2 0.2 fusion.49
  17.4 0.2 fusion.52
  17.7 0.2 fusion.50
  17.9 0.2 fusion.51
  18.1 0.1 maximum_convert_fusion
  18.2 0.1 broadcast_compare_fusion
  18.2 6.4 %copy.17 = bf16[16,128,1024]{1,2,0:T(8,128)(2,1)} copy(bf16[16,128,1024]{2,1,0:T(8,128)(2,1)} %param.23) | data formatting | bytes 8388608 | tf_op args[8]
  24.6 78.4 %all-reduce = (f32[1024]{0:T(1024)S(1)}, f32[16]{0:T(128)S(1)}, f32[16]{0:T(128)S(1)}, f32[2048]{0:T(1024)S(1)}, f32[1024]{0:T(1024)S(1)}, /*index=5*/f32[2048]{0:T(1024)S(1)}) all-reduce(f32[1024]{0:T(1024)S(1)} %bitcast.74, f32[16]{0:T(128)S(1)} %get-tuple-element.8, ...), channel_id=1, replica_groups=mesh['kv'=16,'tp'=2] {'kv'}, use_global_device_ids=true, to_apply=%region_7.0 | all-reduce | flops 6176 | bytes 49408 | tf_op jit(solution)/shard_map/psum | solution.py:80
  103.1 0.1 multiply_cosine_fusion
  103.2 25.6 %all-reduce.4.cloned.1.call-done = (f32[16,1024]{1,0:T(8,128)}, f32[16,2048]{1,0:T(8,128)}, f32[16,1024]{1,0:T(8,128)}, f32[16,2048]{1,0:T(8,128)}) async-done(((f32[16,1024]{1,0:T(8,128)}, f32[16,2048]{1,0:T(8,128)}, f32[16,1024]{1,0:T(8,128)}, f32[16,2048]{1,0:T(8,128)}), (f32[16,1024]{1,0:T(8,128)}, f32[16,2048]{1,0:T(8,128)}, f32[16,1024]{1,0:T(8,128)}, ...) | async-done | bytes 393232 | tf_op jit(solution)/shard_map/psum | solution.py:80
  128.8 1.0 subtract_multiply_fusion
  129.7 0.1 reshape.189
  129.8 0.1 reshape.192
  129.9 0.2 subtract_convert_fusion
  130.1 0.1 fusion.37
  130.2 3.4 fusion.19
  133.5 0.1 fusion.23
  133.7 6.4 %fusion = f32[16,16,1,128]{3,2,1,0:T(1,128)} fusion(bf16[16,16,128,1]{2,1,0,3:T(8,128)(2,1)S(1)} %fusion.23, bf16[16,128,2048]{2,1,0:T(8,128)(2,1)} %param.24), kind=kOutput, calls=%fused_computation | convolution fusion | flops 8388608 | bytes 8585216 | tf_op jit(solution)/shard_map/bhj,bjhe->bhe/dot_general | solution.py:114
  140.2 0.1 convert_bitcast_fusion
  140.3 0.2 multiply_reduce_fusion.1
  140.5 0.1 bitcast_multiply_fusion
  140.6 59.1 %all-gather.3.cloned.1.call-done = f32[256,16,128]{2,1,0:T(8,128)} async-done(((f32[16,16,128]{2,1,0:T(8,128)}), f32[256,16,128]{2,1,0:T(8,128)}) %all-gather.3.cloned.1.call-update) | async-done | bytes 2097168 | tf_op jit(solution)/shard_map/all_gather | solution.py:117
  199.7 1.7 reduce_sum.76
  201.5 0.1 fusion.48
  201.6 0.2 multiply_reduce_fusion
  201.8 0.1 mul.338
  201.9 0.1 sub.65
  202.0 0.1 mul.330
  202.1 0.4 convolution_convert_fusion
  202.6 0.7 copy.23
  203.4 2.8 fusion.53
  206.2 3.6 %reduce-scatter.10.cloned.1.call-done = bf16[128,16]{1,0:T(8,128)(2,1)} async-done(((bf16[256,16]{1,0:T(8,128)(2,1)}), bf16[128,16]{1,0:T(8,128)(2,1)}) %reduce-scatter.10.cloned.1.call-update) | async-done | bytes 4112
  209.8 0.8 copy.24
  210.7 42.0 %all_gather.15 = bf16[16,4096]{1,0:T(8,128)(2,1)S(1)} all-gather(bf16[16,128]{1,0:T(8,128)(2,1)S(1)} %add_convert_fusion.3), channel_id=1, replica_groups=mesh['kv'=16,'tp'=2] {'kv','tp'}, dimensions={1}, use_global_device_ids=true | all-gather | bytes 135168 | tf_op jit(solution)/shard_map/all_gather | solution.py:139
  252.7 0.2 fusion.8
  252.8 5.5 %fusion.7 = f32[16,4096]{1,0:T(8,128)} fusion(bf16[512,4096]{1,0:T(8,128)(2,1)} %param.29, bf16[4096,512]{1,0:T(8,128)(2,1)} %param.28, bf16[16,4096]{1,0:T(8,128)(2,1)S(1)} %all_gather.15, f32[4096]{0:T(1024)S(1)} %convert_element_type.105, f32[512]{0:T(512)S(1)} %bitcast.76, f32[16]{0:T(128)S(1)} %get-tuple-element.32, f32[16]{0:T(128)S(1)} %get-tuple-element.31), kind=kOutput, calls=%fused_computation.8 | convolution fusion | flops 134463488 | bytes 8800384 | tf_op jit(solution)/shard_map/dot_general | solution.py:153
  258.4 73.3 %reduce-scatter.6.cloned.1.call-done = f32[16,256]{1,0:T(8,128)} async-done(((f32[16,4096]{1,0:T(8,128)}), f32[16,256]{1,0:T(8,128)}) %reduce-scatter.6.cloned.1.call-update) | async-done | bytes 16400 | tf_op jit(solution)/shard_map/reduce_scatter | solution.py:154
  331.7 5.9 %reduce-scatter.8.cloned.1.call-done = f32[16,128]{1,0:T(8,128)} async-done(((f32[16,256]{1,0:T(8,128)}), f32[16,128]{1,0:T(8,128)}) %reduce-scatter.8.cloned.1.call-update) | async-done | bytes 8208 | tf_op jit(solution)/shard_map/reduce_scatter | solution.py:155
  337.6 1.3 add_convert_fusion.2
  (47 shorter events, 0.4 us)
Async XLA Ops:
  6.5 5.2 %copy-start = (bf16[256,2048]{1,0:T(8,128)(2,1)S(1)}, bf16[256,2048]{1,0:T(8,128)(2,1)}, u32[]{:S(2)}) copy-start(bf16[256,2048]{1,0:T(8,128)(2,1)} %param.21) | copy-start | bytes 3145732
  6.5 10.9 %copy-start.1 = (bf16[256,2048]{1,0:T(8,128)(2,1)S(1)}, bf16[256,2048]{1,0:T(8,128)(2,1)}, u32[]{:S(2)}) copy-start(bf16[256,2048]{1,0:T(8,128)(2,1)} %param.20) | copy-start | bytes 3145732
  6.5 11.3 %copy-start.3 = (bf16[256,1024]{1,0:T(8,128)(2,1)S(1)}, bf16[256,1024]{1,0:T(8,128)(2,1)}, u32[]{:S(2)}) copy-start(bf16[256,1024]{1,0:T(8,128)(2,1)} %param.19) | copy-start | bytes 1572868
  6.5 11.1 %copy-start.2 = (bf16[256,1024]{1,0:T(8,128)(2,1)S(1)}, bf16[256,1024]{1,0:T(8,128)(2,1)}, u32[]{:S(2)}) copy-start(bf16[256,1024]{1,0:T(8,128)(2,1)} %param.18) | copy-start | bytes 1572868
  6.5 11.5 %copy-start.10 = (s32[16]{0:T(128)S(1)}, s32[16]{0:T(128)}, u32[]{:S(2)}) copy-start(s32[16]{0:T(128)} %param.16) | copy-start | bytes 196
  6.5 122.2 %all-reduce.4.cloned.1.call-start = ((), (), s32[]{:S(2)}) async-start(), calls=%async_computation.7 | async-start | bytes 786432 | tf_op jit(solution)/shard_map/psum | solution.py:80
  16.3 183.4 %all-gather.3.cloned.1.call-start = ((), (), s32[]{:S(2)}) async-start(), calls=%async_computation.5 | async-start | bytes 2228224 | tf_op jit(solution)/shard_map/all_gather | solution.py:117
  18.2 6.4 %copy-start.11 = (f32[16]{0:T(128)S(1)}, f32[16]{0:T(128)}, u32[]{:S(2)}) copy-start(f32[16]{0:T(128)} %param.22) | copy-start | bytes 196
  133.7 6.5 %copy-start.9 = (bf16[2048]{0:T(1024)(128)(2,1)S(1)}, bf16[2048]{0:T(1024)(128)(2,1)}, u32[]{:S(2)}) copy-start(bf16[2048]{0:T(1024)(128)(2,1)} %param.25) | copy-start | bytes 12292
  133.7 6.5 %copy-start.7 = (bf16[4096]{0:T(1024)(128)(2,1)S(1)}, bf16[4096]{0:T(1024)(128)(2,1)}, u32[]{:S(2)}) copy-start(bf16[4096]{0:T(1024)(128)(2,1)} %param.27) | copy-start | bytes 24580
  133.7 6.5 %copy-start.5 = (f32[16,2048]{1,0:T(8,128)S(1)}, f32[16,2048]{1,0:T(8,128)}, u32[]{:S(2)}) copy-start(f32[16,2048]{1,0:T(8,128)} %get-tuple-element.16) | copy-start | bytes 393220
  140.1 62.1 %copy-start.4 = (bf16[2048,256]{1,0:T(8,128)(2,1)S(1)}, bf16[2048,256]{1,0:T(8,128)(2,1)}, u32[]{:S(2)}) copy-start(bf16[2048,256]{1,0:T(8,128)(2,1)} %param.26) | copy-start | bytes 3145732
  140.1 62.1 %copy-start.6 = (f32[16,2048]{1,0:T(8,128)S(1)}, f32[16,2048]{1,0:T(8,128)}, u32[]{:S(2)}) copy-start(f32[16,2048]{1,0:T(8,128)} %get-tuple-element.18) | copy-start | bytes 393220
  140.1 69.7 %reduce-scatter.10.cloned.1.call-start = ((), (), s32[]{:S(2)}) async-start(), calls=%async_computation.6 | async-start | bytes 98304
  201.5 9.2 %copy-start.8 = (bf16[16,128]{1,0:T(8,128)(2,1)S(1)}, bf16[16,128]{1,0:T(8,128)(2,1)}, u32[]{:S(2)}) copy-start(bf16[16,128]{1,0:T(8,128)(2,1)} %param.15) | copy-start | bytes 12292
  203.3 128.3 %reduce-scatter.6.cloned.1.call-start = ((), (), s32[]{:S(2)}) async-start(), calls=%async_computation.3 | async-start | bytes 278528 | tf_op jit(solution)/shard_map/reduce_scatter | solution.py:154
  258.3 79.3 %reduce-scatter.8.cloned.1.call-start = ((), (), s32[]{:S(2)}) async-start(), calls=%async_computation.4 | async-start | bytes 24576 | tf_op jit(solution)/shard_map/reduce_scatter | solution.py:155
Sparse Core Ops, SparseCore 0:
  16.5 112.2 all-reduce.3
  140.2 59.4 all-gather.2
  203.5 6.3 reduce-scatter.9
  258.4 73.1 reduce-scatter.5
  333.7 3.8 reduce-scatter.7
